TPU v7x, 32 devices: a whole 2x2x4 slice. The times are simulated.
32 devices in a mesh: sp: 4 (over z), dp: 8 (over y, x, core).
Axes of the slice: x: 2, y: 2, z: 4, core: 2. Of those that a mesh axis runs over, the one named last changes fastest.
Arguments:
- tokens: bfloat16 [16, 256, 1024], P('dp', 'sp'), may hold values from -6 to 6
- norm_gain: float32 [1024], replicated, may hold values from 0.1 to 1.9
- w_query: bfloat16 [1024, 128], P('dp'), may hold values from -0.1875 to 0.1875
- w_key: bfloat16 [1024, 128], P('dp'), may hold values from -0.1875 to 0.1875
- w_value: bfloat16 [1024, 128], P('dp'), may hold values from -0.1875 to 0.1875
- w_rank_forward: bfloat16 [1024, 16], P('dp'), may hold values from -0.1875 to 0.1875
- w_rank_backward: bfloat16 [1024, 16], P('dp'), may hold values from -0.1875 to 0.1875
- up_forward: bfloat16 [16, 128], replicated, may hold values from -1.5 to 1.5
- up_backward: bfloat16 [16, 128], replicated, may hold values from -1.5 to 1.5
- bias_forward: float32 [128], replicated, may hold values from -1.5 to 3
- bias_backward: float32 [128], replicated, may hold values from -1.5 to 3
- out_gain: float32 [32], replicated, may hold values from 0.1 to 1.9
- w_out: bfloat16 [128, 1024], P('dp'), may hold values from -0.5 to 0.5
Outputs:
- mixed_out: bfloat16 [16, 256, 1024], P('dp', 'sp')
All inputs are finite; a program needn't handle non-finite values.
Results may differ from a plain program's by a relative error of at most 0.005.
Values may be sent and summed in bfloat16 or wider, within the bound.
A program may use at most 64 MiB of HBM per device.

v0:
```python
import jax
import jax.numpy as jnp
from jax import lax
from jax.sharding import PartitionSpec as P

HK = 32
HV = 32
BLOCK = 64
eps = 1e-06
precise = lax.Precision.HIGHEST


def over_all(x, axis, dim, take_in, carry):
    whole = jax.tree.map(lambda part: lax.all_gather(part, axis, axis=dim, tiled=True), x)
    return take_in(carry, whole, jnp.int32(0))


def for_sending(x):
    return jax.tree.map(lambda a: a.astype(jnp.bfloat16) if a.dtype == jnp.float32 else a, x)


def rms_norm(values, norm_scale):
    return values * lax.rsqrt(jnp.mean(values * values, axis=-1, keepdims=True) + eps) * norm_scale


def one_way(queries, key_rows, value_rows, decay_rates):
    head_count, length, key_width = queries.shape
    value_width = value_rows.shape[-1]
    blocks = length // BLOCK

    def in_blocks(tensor):
        return tensor.reshape(head_count, blocks, BLOCK, tensor.shape[-1])

    query_blocks = in_blocks(queries)
    key_blocks = in_blocks(key_rows)
    value_blocks = in_blocks(value_rows)
    running = jnp.cumsum(in_blocks(decay_rates), axis=2)
    closing = running[:, :, -1:, :]
    query_decayed = query_blocks * jnp.exp(running)
    key_inverse = key_blocks * jnp.exp(-running)
    key_remain = key_blocks * jnp.exp(closing - running)
    triangle = jnp.tril(jnp.ones((BLOCK, BLOCK), jnp.float32))
    scores = jnp.einsum("hnid,hnjd->hnij", query_decayed, key_inverse, precision=precise) * triangle
    within = jnp.einsum("hnij,hnjv->hniv", scores, value_blocks, precision=precise)
    block_decay = jnp.exp(closing[:, :, 0, :])

    def advance(carried, inputs):
        query_now, key_now, value_now, decay_now = inputs
        emitted = jnp.einsum("hid,hdv->hiv", query_now, carried, precision=precise)
        carried = decay_now[..., None] * carried + jnp.einsum(
            "hid,hiv->hdv", key_now, value_now, precision=precise
        )
        return (carried, emitted)

    initial = jnp.zeros((head_count, key_width, value_width), jnp.float32)
    stacked = tuple(
        (
            jnp.moveaxis(tensor, 1, 0)
            for tensor in (query_decayed, key_remain, value_blocks, block_decay)
        )
    )
    final_state, across = lax.scan(advance, initial, stacked)
    return (within + jnp.moveaxis(across, 0, 1)).reshape(head_count, length, value_width)


def both_ways(queries, key_rows, value_rows, rates_forward, rates_backward):
    forward = one_way(queries, key_rows, value_rows, rates_forward)
    backward = one_way(
        jnp.flip(queries, 1),
        jnp.flip(key_rows, 1),
        jnp.flip(value_rows, 1),
        jnp.flip(rates_backward, 1),
    )
    return forward + jnp.flip(backward, 1)


def by_head(tensor, head_width):
    length = tensor.shape[0]
    return tensor.reshape(length, -1, head_width).transpose(1, 0, 2).astype(jnp.float32)


def attend(queries, key_rows, value_rows, rates_forward, rates_backward, out_gain):
    combined = both_ways(
        by_head(queries, HK) * HK ** (-0.5),
        by_head(key_rows, HK),
        by_head(value_rows, HV),
        by_head(rates_forward, HK),
        by_head(rates_backward, HK),
    )
    normed = rms_norm(combined, out_gain).astype(jnp.bfloat16)
    return normed.transpose(1, 0, 2).reshape(normed.shape[1], -1)


def per_device(
    tokens,
    norm_gain,
    w_query,
    w_key,
    w_value,
    w_rank_forward,
    w_rank_backward,
    up_forward,
    up_backward,
    bias_forward,
    bias_backward,
    out_gain,
    w_out,
):
    seq_local, tok_local, model_width = tokens.shape
    sp_count = lax.axis_size("sp")
    length = tok_local * sp_count
    rate_scale = 2.0 / length
    row_count = seq_local * tok_local
    normed = rms_norm(tokens.reshape(row_count, model_width).astype(jnp.float32), norm_gain).astype(
        jnp.bfloat16
    )

    def add_rows(totals, pieces, offset):
        span_rows = pieces[0].shape[0]
        left_part = lax.dynamic_slice_in_dim(normed, offset, span_rows, 1)
        return tuple(
            (
                running_sum + jnp.dot(left_part, shard_piece, preferred_element_type=jnp.float32)
                for running_sum, shard_piece in zip(totals, pieces)
            )
        )

    starting = tuple(
        (
            jnp.zeros((row_count, weight.shape[1]), jnp.float32)
            for weight in (w_query, w_key, w_value, w_rank_forward, w_rank_backward)
        )
    )
    projected = over_all(
        (w_query, w_key, w_value, w_rank_forward, w_rank_backward), "dp", 0, add_rows, starting
    )
    queries = projected[0].astype(jnp.bfloat16).reshape(seq_local, tok_local, -1)
    key_rows = projected[1].astype(jnp.bfloat16).reshape(seq_local, tok_local, -1)
    value_rows = projected[2].astype(jnp.bfloat16).reshape(seq_local, tok_local, -1)
    rank_forward = projected[3].astype(jnp.bfloat16)
    rank_backward = projected[4].astype(jnp.bfloat16)
    head_queries, head_keys, head_values = (
        lax.all_to_all(queries, "sp", split_axis=2, concat_axis=1, tiled=True),
        lax.all_to_all(key_rows, "sp", split_axis=2, concat_axis=1, tiled=True),
        lax.all_to_all(value_rows, "sp", split_axis=2, concat_axis=1, tiled=True),
    )
    own_forward = (
        jax.nn.log_sigmoid(
            jnp.dot(rank_forward, up_forward, preferred_element_type=jnp.float32) + bias_forward
        )
        * rate_scale
    )
    own_backward = (
        jax.nn.log_sigmoid(
            jnp.dot(rank_backward, up_backward, preferred_element_type=jnp.float32) + bias_backward
        )
        * rate_scale
    )
    rates_forward, rates_backward = (
        lax.all_to_all(
            for_sending(own_forward.reshape(seq_local, tok_local, -1)),
            "sp",
            split_axis=2,
            concat_axis=1,
            tiled=True,
        ),
        lax.all_to_all(
            for_sending(own_backward.reshape(seq_local, tok_local, -1)),
            "sp",
            split_axis=2,
            concat_axis=1,
            tiled=True,
        ),
    )
    attended = jax.vmap(attend, in_axes=(0, 0, 0, 0, 0, None))(
        head_queries, head_keys, head_values, rates_forward, rates_backward, out_gain
    )
    gathered_heads = jax.tree.map(
        lambda part, own: part.astype(own.dtype),
        lax.all_to_all(for_sending(attended), "sp", split_axis=1, concat_axis=2, tiled=True),
        attended,
    ).reshape(row_count, -1)

    def add_out(running_sum, shard_piece, offset):
        left_part = lax.dynamic_slice_in_dim(gathered_heads, offset, shard_piece.shape[0], 1)
        return running_sum + jnp.dot(left_part, shard_piece, preferred_element_type=jnp.float32)

    mixed_out = over_all(
        w_out, "dp", 0, add_out, jnp.zeros((row_count, w_out.shape[1]), jnp.float32)
    )
    return mixed_out.astype(jnp.bfloat16).reshape(seq_local, tok_local, -1)


def solution(mesh):
    return jax.shard_map(
        per_device,
        mesh=mesh,
        in_specs=(
            P("dp", "sp", None),
            P(),
            P("dp", None),
            P("dp", None),
            P("dp", None),
            P("dp", None),
            P("dp", None),
            P(),
            P(),
            P(),
            P(),
            P(),
            P("dp", None),
        ),
        out_specs=P("dp", "sp", None),
        check_vma=False,
    )
```

profile of v0, /device:TPU:0, one launch (start us, length us, event | category | flops | bytes accessed | tf_op | source)
XLA Modules:
  0.0 118.0 jit_solution(11206527147901036018)
XLA Ops:
  0.0 1.2 multiply_reduce_fusion
  1.3 11.1 %all_gather.18 = bf16[1024,128]{1,0:T(8,128)(2,1)S(1)} all-gather(bf16[128,128]{1,0:T(8,128)(2,1)} %param.19), channel_id=1, replica_groups=mesh['sp'=4,'dp'=8] {'dp'}, dimensions={0}, use_global_device_ids=true | all-gather | bytes 294912 | tf_op jit(solution)/shard_map/all_gather | solution.py:14
  12.5 0.2 convolution_convert_fusion.3
  12.9 0.7 reshape.393
  13.6 5.0 %all-to-all-start = ((bf16[4,2,2048]{2,1,0:T(2,128)(2,1)}), bf16[4,2,2048]{2,1,0:T(2,128)(2,1)S(1)}, u32[]{:S(2)}, u32[]{:S(2)}) async-start(bf16[4,2,2048]{2,1,0:T(2,128)(2,1)} %reshape.393), calls=%async_computation | async-start | bytes 65536 | tf_op jit(solution)/shard_map/all_to_all | solution.py:143
  18.6 9.0 %all_gather.20 = bf16[1024,128]{1,0:T(8,128)(2,1)S(1)} all-gather(bf16[128,128]{1,0:T(8,128)(2,1)S(1)} %copy-done.2), channel_id=1, replica_groups=mesh['sp'=4,'dp'=8] {'dp'}, dimensions={0}, use_global_device_ids=true | all-gather | bytes 294912 | tf_op jit(solution)/shard_map/all_gather | solution.py:14
  27.9 0.5 copy-done.6
  28.3 8.2 %all_gather.19 = bf16[1024,16]{0,1:T(8,128)(2,1)S(1)} all-gather(bf16[128,16]{0,1:T(8,128)(2,1)S(1)} %copy-done.6), channel_id=1, replica_groups=mesh['sp'=4,'dp'=8] {'dp'}, dimensions={0}, use_global_device_ids=true | all-gather | bytes 36864 | tf_op jit(solution)/shard_map/all_gather | solution.py:14
  36.6 9.0 %all_gather.21 = bf16[1024,128]{1,0:T(8,128)(2,1)S(1)} all-gather(bf16[128,128]{1,0:T(8,128)(2,1)S(1)} %copy-done.3), channel_id=1, replica_groups=mesh['sp'=4,'dp'=8] {'dp'}, dimensions={0}, use_global_device_ids=true | all-gather | bytes 294912 | tf_op jit(solution)/shard_map/all_gather | solution.py:14
  45.6 0.2 convolution_convert_fusion.1
  45.9 0.5 copy-done.7
  46.3 8.2 %all_gather.22 = bf16[1024,16]{0,1:T(8,128)(2,1)S(1)} all-gather(bf16[128,16]{0,1:T(8,128)(2,1)S(1)} %copy-done.7), channel_id=1, replica_groups=mesh['sp'=4,'dp'=8] {'dp'}, dimensions={0}, use_global_device_ids=true | all-gather | bytes 36864 | tf_op jit(solution)/shard_map/all_gather | solution.py:14
  54.6 0.4 fusion.47
  55.0 0.3 copy-done.9
  55.2 0.4 fusion.50
  55.8 0.7 reshape.389
  56.7 0.7 reshape.391
  57.5 0.7 reshape.387
  58.4 0.7 reshape.395
  59.1 5.1 %all-to-all-start.1 = ((bf16[4,2,2048]{2,1,0:T(2,128)(2,1)}), bf16[4,2,2048]{2,1,0:T(2,128)(2,1)S(1)}, u32[]{:S(2)}, u32[]{:S(2)}) async-start(bf16[4,2,2048]{2,1,0:T(2,128)(2,1)} %reshape.391), calls=%async_computation.1 | async-start | bytes 65536 | tf_op jit(solution)/shard_map/all_to_all | solution.py:160
  64.3 5.5 %all-to-all-done.1 = bf16[4,2,2048]{2,1,0:T(2,128)(2,1)S(1)} async-done(((bf16[4,2,2048]{2,1,0:T(2,128)(2,1)}), bf16[4,2,2048]{2,1,0:T(2,128)(2,1)S(1)}, u32[]{:S(2)}, u32[]{:S(2)}) %all-to-all-start.1) | async-done | bytes 32800 | tf_op jit(solution)/shard_map/all_to_all | solution.py:160
  69.9 3.3 %all-to-all-start.2 = ((bf16[4,2,2048]{2,1,0:T(2,128)(2,1)}), bf16[4,2,2048]{2,1,0:T(2,128)(2,1)S(1)}, u32[]{:S(2)}, u32[]{:S(2)}) async-start(bf16[4,2,2048]{2,1,0:T(2,128)(2,1)} %reshape.389), calls=%async_computation.2 | async-start | bytes 65536 | tf_op jit(solution)/shard_map/all_to_all | solution.py:144
  73.3 5.5 %all-to-all-done.2 = bf16[4,2,2048]{2,1,0:T(2,128)(2,1)S(1)} async-done(((bf16[4,2,2048]{2,1,0:T(2,128)(2,1)}), bf16[4,2,2048]{2,1,0:T(2,128)(2,1)S(1)}, u32[]{:S(2)}, u32[]{:S(2)}) %all-to-all-start.2) | async-done | bytes 32800 | tf_op jit(solution)/shard_map/all_to_all | solution.py:144
  78.8 3.3 %all-to-all-start.3 = ((bf16[4,2,2048]{2,1,0:T(2,128)(2,1)}), bf16[4,2,2048]{2,1,0:T(2,128)(2,1)S(1)}, u32[]{:S(2)}, u32[]{:S(2)}) async-start(bf16[4,2,2048]{2,1,0:T(2,128)(2,1)} %reshape.387), calls=%async_computation.3 | async-start | bytes 65536 | tf_op jit(solution)/shard_map/all_to_all | solution.py:145
  82.6 5.1 %all-to-all-done.3 = bf16[4,2,2048]{2,1,0:T(2,128)(2,1)S(1)} async-done(((bf16[4,2,2048]{2,1,0:T(2,128)(2,1)}), bf16[4,2,2048]{2,1,0:T(2,128)(2,1)S(1)}, u32[]{:S(2)}, u32[]{:S(2)}) %all-to-all-start.3) | async-done | bytes 32800 | tf_op jit(solution)/shard_map/all_to_all | solution.py:145
  87.7 3.3 %all-to-all-start.4 = ((bf16[4,2,2048]{2,1,0:T(2,128)(2,1)}), bf16[4,2,2048]{2,1,0:T(2,128)(2,1)S(1)}, u32[]{:S(2)}, u32[]{:S(2)}) async-start(bf16[4,2,2048]{2,1,0:T(2,128)(2,1)} %reshape.395), calls=%async_computation.4 | async-start | bytes 65536 | tf_op jit(solution)/shard_map/all_to_all | solution.py:167
  91.1 0.3 reduce_window_sum.19
  91.3 0.6 convolution_multiply_fusion.1
  92.3 1.8 %while.26 = (s32[]{:T(128)}, f32[2,1,32,32]{3,2,0,1:T(8,128)S(1)}, f32[4,2,1,64,32]{3,4,0,1,2:T(8,128)S(1)}, f32[4,2,1,32]{3,0,1,2:T(4,128)S(1)}, f32[4,2,1,64,3...) while((s32[]{:T(128)}, f32[2,1,32,32]{3,2,0,1:T(8,128)S(1)}, ...), condition=%wide.region_3.4_spmd.clone, body=%wide.region_2.3_spmd.clone.sunk | while | flops 3153923 | bytes 209522 | solution.py:62
  92.3 0.2 fusion.90
  92.8 0.2 fusion.90
  93.2 0.2 fusion.90
  93.7 0.2 fusion.90
  94.5 0.3 fusion.28
  95.9 0.6 all-to-all-done.4
  97.2 0.3 reduce_window_sum.21
  97.9 2.0 %while.27 = (s32[]{:T(128)}, f32[2,1,32,32]{3,2,0,1:T(8,128)S(1)}, f32[4,2,1,64,32]{3,4,0,1,2:T(8,128)S(1)}, f32[4,2,1,32]{3,0,1,2:T(4,128)S(1)}, f32[4,2,1,64,3...) while((s32[]{:T(128)}, f32[2,1,32,32]{3,2,0,1:T(8,128)S(1)}, ...), condition=%wide.region_6.7_spmd.clone, body=%wide.region_5.6_spmd.clone.sunk | while | flops 3153923 | bytes 240763 | solution.py:62
  97.9 0.2 fusion.96
  98.4 0.2 fusion.96
  98.9 0.2 fusion.96
  99.3 0.2 fusion.96
  99.8 0.6 convolution_multiply_fusion
  100.4 0.5 fusion.29
  101.4 0.6 copy-done.8
  102.3 0.8 reshape.397
  103.1 4.6 %all-to-all-start.5 = ((bf16[4,2,2048]{2,1,0:T(2,128)(2,1)}), bf16[4,2,2048]{2,1,0:T(2,128)(2,1)S(1)}, u32[]{:S(2)}, u32[]{:S(2)}) async-start(bf16[4,2,2048]{2,1,0:T(2,128)(2,1)} %reshape.397), calls=%async_computation.5 | async-start | bytes 65536 | tf_op jit(solution)/shard_map/all_to_all | solution.py:180
  107.7 9.0 %all_gather.23 = bf16[128,1024]{1,0:T(8,128)(2,1)S(1)} all-gather(bf16[16,1024]{1,0:T(8,128)(2,1)S(1)} %copy-done.4), channel_id=1, replica_groups=mesh['sp'=4,'dp'=8] {'dp'}, dimensions={0}, use_global_device_ids=true | all-gather | bytes 294912 | tf_op jit(solution)/shard_map/all_gather | solution.py:14
  117.1 1.0 convolution_convert_fusion
  (108 shorter events, 7.3 us)
Async XLA Ops:
  0.0 54.5 %copy-start = (bf16[16,128]{1,0:T(8,128)(2,1)S(1)}, bf16[16,128]{1,0:T(8,128)(2,1)}, u32[]{:S(2)}) copy-start(bf16[16,128]{1,0:T(8,128)(2,1)} %param.24) | copy-start | bytes 12292
  0.0 12.4 %copy-start.1 = (bf16[2,64,1024]{2,1,0:T(8,128)(2,1)S(1)}, bf16[2,64,1024]{2,1,0:T(8,128)(2,1)}, u32[]{:S(2)}) copy-start(bf16[2,64,1024]{2,1,0:T(8,128)(2,1)} %param.17) | copy-start | bytes 786436
  1.3 11.1 %copy-start.5 = (f32[1024]{0:T(1024)S(1)}, f32[1024]{0:T(1024)}, u32[]{:S(2)}) copy-start(f32[1024]{0:T(1024)} %param.18) | copy-start | bytes 12292
  13.6 5.0 %copy-start.2 = (bf16[128,128]{1,0:T(8,128)(2,1)S(1)}, bf16[128,128]{1,0:T(8,128)(2,1)}, u32[]{:S(2)}) copy-start(bf16[128,128]{1,0:T(8,128)(2,1)} %param.20) | copy-start | bytes 98308
  13.6 45.5 %all-to-all-start = ((bf16[4,2,2048]{2,1,0:T(2,128)(2,1)}), bf16[4,2,2048]{2,1,0:T(2,128)(2,1)S(1)}, u32[]{:S(2)}, u32[]{:S(2)}) async-start(bf16[4,2,2048]{2,1,0:T(2,128)(2,1)} %reshape.393), calls=%async_computation | async-start | bytes 65536 | tf_op jit(solution)/shard_map/all_to_all | solution.py:143
  27.7 0.7 copy-start.6
  28.3 8.2 %copy-start.3 = (bf16[128,128]{1,0:T(8,128)(2,1)S(1)}, bf16[128,128]{1,0:T(8,128)(2,1)}, u32[]{:S(2)}) copy-start(bf16[128,128]{1,0:T(8,128)(2,1)} %param.21) | copy-start | bytes 98308
  45.6 0.7 copy-start.7
  46.3 8.2 %copy-start.10 = (f32[128]{0:T(128)S(1)}, f32[128]{0:T(128)}, u32[]{:S(2)}) copy-start(f32[128]{0:T(128)} %param.26) | copy-start | bytes 1540
  54.6 0.7 copy-start.9
  54.6 0.7 copy-start.11
  59.1 10.7 %all-to-all-start.1 = ((bf16[4,2,2048]{2,1,0:T(2,128)(2,1)}), bf16[4,2,2048]{2,1,0:T(2,128)(2,1)S(1)}, u32[]{:S(2)}, u32[]{:S(2)}) async-start(bf16[4,2,2048]{2,1,0:T(2,128)(2,1)} %reshape.391), calls=%async_computation.1 | async-start | bytes 65536 | tf_op jit(solution)/shard_map/all_to_all | solution.py:160
  69.9 8.9 %all-to-all-start.2 = ((bf16[4,2,2048]{2,1,0:T(2,128)(2,1)}), bf16[4,2,2048]{2,1,0:T(2,128)(2,1)S(1)}, u32[]{:S(2)}, u32[]{:S(2)}) async-start(bf16[4,2,2048]{2,1,0:T(2,128)(2,1)} %reshape.389), calls=%async_computation.2 | async-start | bytes 65536 | tf_op jit(solution)/shard_map/all_to_all | solution.py:144
  78.8 8.9 %all-to-all-start.3 = ((bf16[4,2,2048]{2,1,0:T(2,128)(2,1)}), bf16[4,2,2048]{2,1,0:T(2,128)(2,1)S(1)}, u32[]{:S(2)}, u32[]{:S(2)}) async-start(bf16[4,2,2048]{2,1,0:T(2,128)(2,1)} %reshape.387), calls=%async_computation.3 | async-start | bytes 65536 | tf_op jit(solution)/shard_map/all_to_all | solution.py:145
  87.7 8.9 %all-to-all-start.4 = ((bf16[4,2,2048]{2,1,0:T(2,128)(2,1)}), bf16[4,2,2048]{2,1,0:T(2,128)(2,1)S(1)}, u32[]{:S(2)}, u32[]{:S(2)}) async-start(bf16[4,2,2048]{2,1,0:T(2,128)(2,1)} %reshape.395), calls=%async_computation.4 | async-start | bytes 65536 | tf_op jit(solution)/shard_map/all_to_all | solution.py:167
  101.4 0.7 copy-start.8
  103.1 4.6 %copy-start.4 = (bf16[16,1024]{1,0:T(8,128)(2,1)S(1)}, bf16[16,1024]{1,0:T(8,128)(2,1)}, u32[]{:S(2)}) copy-start(bf16[16,1024]{1,0:T(8,128)(2,1)} %param.29) | copy-start | bytes 98308
  103.1 13.7 %all-to-all-start.5 = ((bf16[4,2,2048]{2,1,0:T(2,128)(2,1)}), bf16[4,2,2048]{2,1,0:T(2,128)(2,1)S(1)}, u32[]{:S(2)}, u32[]{:S(2)}) async-start(bf16[4,2,2048]{2,1,0:T(2,128)(2,1)} %reshape.397), calls=%async_computation.5 | async-start | bytes 65536 | tf_op jit(solution)/shard_map/all_to_all | solution.py:180
where the time goes:
time: 119 us; the launch traced here: 118 us
  blocking collectives  54.7 us (46%)
  starting transfers between devices  24.5 us (21%)
  waiting for transfers between devices  16.7 us (14%)
  local copies, waits for them, and re-layouts  11.5 us (10%)
  matrix products  7.71 us (6%)
  other arithmetic  2.15 us (2%)
    all_gather x6, blocking collectives, over_all(): lax.all_gather(part, axis, axis=dim, tiled=True)  54.7 us
    unnamed x40, local copies, waits for them, and re-layouts  7.46 us
    all_to_all x1, waiting for transfers between devices, per_device(): lax.all_to_all(for_sending(own_forward.reshape(seq_local, tok_local, -1))...  5.52 us
    all_to_all x1, waiting for transfers between devices, per_device(): lax.all_to_all(key_rows, 'sp', split_axis=2, concat_axis=1, tiled=True)  5.47 us
    all_to_all x1, starting transfers between devices, per_device(): lax.all_to_all(for_sending(own_forward.reshape(seq_local, tok_local, -1))...  5.09 us
    all_to_all x1, waiting for transfers between devices, per_device(): lax.all_to_all(value_rows, 'sp', split_axis=2, concat_axis=1, tiled=True)  5.08 us
    all_to_all x1, starting transfers between devices, per_device(): lax.all_to_all(queries, 'sp', split_axis=2, concat_axis=1, tiled=True)  5 us
    all_to_all x1, starting transfers between devices, per_device(): lax.all_to_all(for_sending(attended), 'sp', split_axis=1, concat_axis=2,...  4.59 us
  transfers between devices with their start and end apart: 6, of which 4 were waited for; matrix products, arithmetic and copies ran while one was open for 9% of the time, Pallas kernels for 0%

commit v1 on v0

--- a/solution.py
+++ b/solution.py
@@ -106,6 +106,19 @@
     out_gain,
     w_out,
 ):
+
+    def unite_points_on_mesh(local_values, row_dim, axis_k):
+        val = jnp.concatenate(
+            lax.all_to_all(
+                jnp.stack(jnp.split(local_values, lax.axis_size("sp"), row_dim), 0),
+                "sp",
+                split_axis=0,
+                concat_axis=0,
+            ),
+            axis_k,
+        )
+        return val
+
     seq_local, tok_local, model_width = tokens.shape
     sp_count = lax.axis_size("sp")
     length = tok_local * sp_count
@@ -141,7 +154,7 @@
     rank_backward = projected[4].astype(jnp.bfloat16)
     head_queries, head_keys, head_values = (
         lax.all_to_all(queries, "sp", split_axis=2, concat_axis=1, tiled=True),
-        lax.all_to_all(key_rows, "sp", split_axis=2, concat_axis=1, tiled=True),
+        unite_points_on_mesh(key_rows, 2, 1),
         lax.all_to_all(value_rows, "sp", split_axis=2, concat_axis=1, tiled=True),
     )
     own_forward = (

time: 119 us -> 120 us (level)
    unnamed x40 -> x42, local copies, waits for them, and re-layouts: 7.46 us -> 7.82 us
where the time goes in v1:
time: 120 us; the launch traced here: 119 us
  blocking collectives  54.7 us (46%)
  starting transfers between devices  24.4 us (20%)
  waiting for transfers between devices  16.6 us (14%)
  local copies, waits for them, and re-layouts  12.1 us (10%)
  matrix products  7.73 us (6%)
  other arithmetic  2.21 us (2%)
    all_gather x6, blocking collectives, over_all(): lax.all_gather(part, axis, axis=dim, tiled=True)  54.7 us
    unnamed x42, local copies, waits for them, and re-layouts  7.82 us
    all_to_all x1, waiting for transfers between devices, per_device(): lax.all_to_all(for_sending(own_forward.reshape(seq_local, tok_local, -1))...  5.5 us
    all_to_all x1, waiting for transfers between devices, per_device(): lax.all_to_all(value_rows, 'sp', split_axis=2, concat_axis=1, tiled=True)  5.33 us
    all_to_all x1, starting transfers between devices, per_device(): lax.all_to_all(for_sending(own_forward.reshape(seq_local, tok_local, -1))...  5.09 us
    all_to_all x1, waiting for transfers between devices, unite_points_on_mesh(): lax.all_to_all(jnp.stack(jnp.split(local_values, lax.axis_size('sp'), row...  5.07 us
    all_to_all x1, starting transfers between devices, per_device(): lax.all_to_all(queries, 'sp', split_axis=2, concat_axis=1, tiled=True)  5 us
    all_to_all x1, starting transfers between devices, per_device(): lax.all_to_all(for_sending(attended), 'sp', split_axis=1, concat_axis=2,...  4.51 us
  transfers between devices with their start and end apart: 6, of which 4 were waited for; matrix products, arithmetic and copies ran while one was open for 9% of the time, Pallas kernels for 0%

profile of v1, /device:TPU:0, one launch (start us, length us, event | category | flops | bytes accessed | tf_op | source)
XLA Modules:
  0.0 118.5 jit_solution(7105921021685367705)
XLA Ops:
  0.0 1.2 multiply_reduce_fusion
  1.3 11.1 %all_gather.18 = bf16[1024,128]{1,0:T(8,128)(2,1)S(1)} all-gather(bf16[128,128]{1,0:T(8,128)(2,1)} %param.19), channel_id=1, replica_groups=mesh['sp'=4,'dp'=8] {'dp'}, dimensions={0}, use_global_device_ids=true | all-gather | bytes 294912 | tf_op jit(solution)/shard_map/all_gather | solution.py:14
  12.5 0.2 convolution_convert_fusion.3
  12.9 0.7 reshape.386
  13.6 5.0 %all-to-all-start = ((bf16[4,2,2048]{2,1,0:T(2,128)(2,1)}), bf16[4,2,2048]{2,1,0:T(2,128)(2,1)S(1)}, u32[]{:S(2)}, u32[]{:S(2)}) async-start(bf16[4,2,2048]{2,1,0:T(2,128)(2,1)} %reshape.386), calls=%async_computation | async-start | bytes 65536 | tf_op jit(solution)/shard_map/all_to_all | solution.py:156
  18.6 8.8 %all_gather.19 = bf16[1024,16]{0,1:T(8,128)(2,1)S(1)} all-gather(bf16[128,16]{0,1:T(8,128)(2,1)S(1)} %copy-done.6), channel_id=1, replica_groups=mesh['sp'=4,'dp'=8] {'dp'}, dimensions={0}, use_global_device_ids=true | all-gather | bytes 36864 | tf_op jit(solution)/shard_map/all_gather | solution.py:14
  27.4 8.5 %all_gather.20 = bf16[1024,128]{1,0:T(8,128)(2,1)S(1)} all-gather(bf16[128,128]{1,0:T(8,128)(2,1)S(1)} %copy-done.2), channel_id=1, replica_groups=mesh['sp'=4,'dp'=8] {'dp'}, dimensions={0}, use_global_device_ids=true | all-gather | bytes 294912 | tf_op jit(solution)/shard_map/all_gather | solution.py:14
  35.9 0.2 convolution_convert_fusion.2
  36.6 0.7 copy-done.3
  37.3 9.1 %all_gather.21 = bf16[1024,128]{1,0:T(8,128)(2,1)S(1)} all-gather(bf16[128,128]{1,0:T(8,128)(2,1)S(1)} %copy-done.3), channel_id=1, replica_groups=mesh['sp'=4,'dp'=8] {'dp'}, dimensions={0}, use_global_device_ids=true | all-gather | bytes 294912 | tf_op jit(solution)/shard_map/all_gather | solution.py:14
  46.5 0.5 copy-done.7
  47.0 8.2 %all_gather.22 = bf16[1024,16]{0,1:T(8,128)(2,1)S(1)} all-gather(bf16[128,16]{0,1:T(8,128)(2,1)S(1)} %copy-done.7), channel_id=1, replica_groups=mesh['sp'=4,'dp'=8] {'dp'}, dimensions={0}, use_global_device_ids=true | all-gather | bytes 36864 | tf_op jit(solution)/shard_map/all_gather | solution.py:14
  55.2 0.4 fusion.48
  55.6 0.3 copy-done.9
  55.9 0.4 fusion.51
  56.5 0.7 reshape.382
  57.3 0.7 reshape.384
  58.1 0.7 reshape.380
  59.0 0.7 reshape.388
  59.7 5.1 %all-to-all-start.1 = ((bf16[4,2,2048]{2,1,0:T(2,128)(2,1)}), bf16[4,2,2048]{2,1,0:T(2,128)(2,1)S(1)}, u32[]{:S(2)}, u32[]{:S(2)}) async-start(bf16[4,2,2048]{2,1,0:T(2,128)(2,1)} %reshape.382), calls=%async_computation.1 | async-start | bytes 65536 | tf_op jit(solution)/shard_map/all_to_all | solution.py:173
  65.0 5.5 %all-to-all-done.1 = bf16[4,2,2048]{2,1,0:T(2,128)(2,1)S(1)} async-done(((bf16[4,2,2048]{2,1,0:T(2,128)(2,1)}), bf16[4,2,2048]{2,1,0:T(2,128)(2,1)S(1)}, u32[]{:S(2)}, u32[]{:S(2)}) %all-to-all-start.1) | async-done | bytes 32800 | tf_op jit(solution)/shard_map/all_to_all | solution.py:173
  70.5 3.3 %all-to-all-start.3 = ((bf16[4,2,2048]{2,1,0:T(2,128)(2,1)}), bf16[4,2,2048]{2,1,0:T(2,128)(2,1)S(1)}, u32[]{:S(2)}, u32[]{:S(2)}) async-start(bf16[4,2,2048]{2,1,0:T(2,128)(2,1)} %reshape.380), calls=%async_computation.3 | async-start | bytes 65536 | tf_op jit(solution)/shard_map/all_to_all | solution.py:158
  74.0 5.3 %all-to-all-done.3 = bf16[4,2,2048]{2,1,0:T(2,128)(2,1)S(1)} async-done(((bf16[4,2,2048]{2,1,0:T(2,128)(2,1)}), bf16[4,2,2048]{2,1,0:T(2,128)(2,1)S(1)}, u32[]{:S(2)}, u32[]{:S(2)}) %all-to-all-start.3) | async-done | bytes 32800 | tf_op jit(solution)/shard_map/all_to_all | solution.py:158
  79.4 3.3 %all-to-all-start.2 = ((bf16[4,2,2048]{2,1,0:T(2,128)(2,1)}), bf16[4,2,2048]{2,1,0:T(2,128)(2,1)S(1)}, u32[]{:S(2)}, u32[]{:S(2)}) async-start(bf16[4,2,2048]{2,1,0:T(2,128)(2,1)} %reshape.384), calls=%async_computation.2 | async-start | bytes 65536 | tf_op jit(solution)/shard_map/all_to_all | solution.py:112
  82.8 0.3 reduce_window_sum.19
  83.2 5.1 %all-to-all-done.2 = bf16[4,2,2048]{2,1,0:T(2,128)(2,1)S(1)} async-done(((bf16[4,2,2048]{2,1,0:T(2,128)(2,1)}), bf16[4,2,2048]{2,1,0:T(2,128)(2,1)S(1)}, u32[]{:S(2)}, u32[]{:S(2)}) %all-to-all-start.2) | async-done | bytes 32800 | tf_op jit(solution)/shard_map/all_to_all | solution.py:112
  88.3 3.3 %all-to-all-start.4 = ((bf16[4,2,2048]{2,1,0:T(2,128)(2,1)}), bf16[4,2,2048]{2,1,0:T(2,128)(2,1)S(1)}, u32[]{:S(2)}, u32[]{:S(2)}) async-start(bf16[4,2,2048]{2,1,0:T(2,128)(2,1)} %reshape.388), calls=%async_computation.4 | async-start | bytes 65536 | tf_op jit(solution)/shard_map/all_to_all | solution.py:180
  91.8 1.8 %while.26 = (s32[]{:T(128)}, f32[2,1,32,32]{3,2,0,1:T(8,128)S(1)}, f32[4,2,1,64,32]{3,4,0,1,2:T(8,128)S(1)}, f32[4,2,1,32]{3,0,1,2:T(4,128)S(1)}, f32[4,2,1,64,3...) while((s32[]{:T(128)}, f32[2,1,32,32]{3,2,0,1:T(8,128)S(1)}, ...), condition=%wide.region_3.4_spmd.clone, body=%wide.region_2.3_spmd.clone.sunk | while | flops 3153923 | bytes 209522 | solution.py:62
  91.8 0.2 fusion.93
  92.3 0.2 fusion.93
  92.7 0.2 fusion.93
  93.2 0.2 fusion.93
  94.0 0.6 convolution_multiply_fusion.1
  94.6 0.3 fusion.28
  96.5 0.7 all-to-all-done.4
  97.8 0.3 reduce_window_sum.21
  98.5 2.0 %while.27 = (s32[]{:T(128)}, f32[2,1,32,32]{3,2,0,1:T(8,128)S(1)}, f32[4,2,1,64,32]{3,4,0,1,2:T(8,128)S(1)}, f32[4,2,1,32]{3,0,1,2:T(4,128)S(1)}, f32[4,2,1,64,3...) while((s32[]{:T(128)}, f32[2,1,32,32]{3,2,0,1:T(8,128)S(1)}, ...), condition=%wide.region_6.7_spmd.clone, body=%wide.region_5.6_spmd.clone.sunk | while | flops 3153923 | bytes 240763 | solution.py:62
  98.5 0.2 fusion.99
  99.0 0.2 fusion.99
  99.5 0.2 fusion.99
  100.0 0.2 fusion.99
  100.4 0.6 convolution_multiply_fusion
  101.0 0.5 fusion.29
  102.0 0.6 copy-done.8
  102.9 0.8 reshape.390
  103.7 4.5 %all-to-all-start.5 = ((bf16[4,2,2048]{2,1,0:T(2,128)(2,1)}), bf16[4,2,2048]{2,1,0:T(2,128)(2,1)S(1)}, u32[]{:S(2)}, u32[]{:S(2)}) async-start(bf16[4,2,2048]{2,1,0:T(2,128)(2,1)} %reshape.390), calls=%async_computation.5 | async-start | bytes 65536 | tf_op jit(solution)/shard_map/all_to_all | solution.py:193
  108.2 9.0 %all_gather.23 = bf16[128,1024]{1,0:T(8,128)(2,1)S(1)} all-gather(bf16[16,1024]{1,0:T(8,128)(2,1)S(1)} %copy-done.4), channel_id=1, replica_groups=mesh['sp'=4,'dp'=8] {'dp'}, dimensions={0}, use_global_device_ids=true | all-gather | bytes 294912 | tf_op jit(solution)/shard_map/all_gather | solution.py:14
  117.6 1.0 convolution_convert_fusion
  (114 shorter events, 7.8 us)
Async XLA Ops:
  0.0 55.2 %copy-start = (bf16[16,128]{1,0:T(8,128)(2,1)S(1)}, bf16[16,128]{1,0:T(8,128)(2,1)}, u32[]{:S(2)}) copy-start(bf16[16,128]{1,0:T(8,128)(2,1)} %param.24) | copy-start | bytes 12292
  0.0 12.4 %copy-start.1 = (bf16[2,64,1024]{2,1,0:T(8,128)(2,1)S(1)}, bf16[2,64,1024]{2,1,0:T(8,128)(2,1)}, u32[]{:S(2)}) copy-start(bf16[2,64,1024]{2,1,0:T(8,128)(2,1)} %param.17) | copy-start | bytes 786436
  1.3 11.1 %copy-start.5 = (f32[1024]{0:T(1024)S(1)}, f32[1024]{0:T(1024)}, u32[]{:S(2)}) copy-start(f32[1024]{0:T(1024)} %param.18) | copy-start | bytes 12292
  13.6 5.0 %copy-start.6 = (bf16[128,16]{0,1:T(8,128)(2,1)S(1)}, bf16[128,16]{0,1:T(8,128)(2,1)}, u32[]{:S(2)}) copy-start(bf16[128,16]{0,1:T(8,128)(2,1)} %param.22) | copy-start | bytes 12292
  13.6 46.1 %all-to-all-start = ((bf16[4,2,2048]{2,1,0:T(2,128)(2,1)}), bf16[4,2,2048]{2,1,0:T(2,128)(2,1)S(1)}, u32[]{:S(2)}, u32[]{:S(2)}) async-start(bf16[4,2,2048]{2,1,0:T(2,128)(2,1)} %reshape.386), calls=%async_computation | async-start | bytes 65536 | tf_op jit(solution)/shard_map/all_to_all | solution.py:156
  18.6 8.8 %copy-start.2 = (bf16[128,128]{1,0:T(8,128)(2,1)S(1)}, bf16[128,128]{1,0:T(8,128)(2,1)}, u32[]{:S(2)}) copy-start(bf16[128,128]{1,0:T(8,128)(2,1)} %param.20) | copy-start | bytes 98308
  36.5 0.8 copy-start.3
  46.3 0.7 copy-start.7
  47.0 8.2 %copy-start.10 = (f32[128]{0:T(128)S(1)}, f32[128]{0:T(128)}, u32[]{:S(2)}) copy-start(f32[128]{0:T(128)} %param.26) | copy-start | bytes 1540
  55.2 0.7 copy-start.9
  55.2 0.7 copy-start.11
  59.7 10.7 %all-to-all-start.1 = ((bf16[4,2,2048]{2,1,0:T(2,128)(2,1)}), bf16[4,2,2048]{2,1,0:T(2,128)(2,1)S(1)}, u32[]{:S(2)}, u32[]{:S(2)}) async-start(bf16[4,2,2048]{2,1,0:T(2,128)(2,1)} %reshape.382), calls=%async_computation.1 | async-start | bytes 65536 | tf_op jit(solution)/shard_map/all_to_all | solution.py:173
  70.5 8.9 %all-to-all-start.3 = ((bf16[4,2,2048]{2,1,0:T(2,128)(2,1)}), bf16[4,2,2048]{2,1,0:T(2,128)(2,1)S(1)}, u32[]{:S(2)}, u32[]{:S(2)}) async-start(bf16[4,2,2048]{2,1,0:T(2,128)(2,1)} %reshape.380), calls=%async_computation.3 | async-start | bytes 65536 | tf_op jit(solution)/shard_map/all_to_all | solution.py:158
  79.4 8.9 %all-to-all-start.2 = ((bf16[4,2,2048]{2,1,0:T(2,128)(2,1)}), bf16[4,2,2048]{2,1,0:T(2,128)(2,1)S(1)}, u32[]{:S(2)}, u32[]{:S(2)}) async-start(bf16[4,2,2048]{2,1,0:T(2,128)(2,1)} %reshape.384), calls=%async_computation.2 | async-start | bytes 65536 | tf_op jit(solution)/shard_map/all_to_all | solution.py:112
  88.3 8.9 %all-to-all-start.4 = ((bf16[4,2,2048]{2,1,0:T(2,128)(2,1)}), bf16[4,2,2048]{2,1,0:T(2,128)(2,1)S(1)}, u32[]{:S(2)}, u32[]{:S(2)}) async-start(bf16[4,2,2048]{2,1,0:T(2,128)(2,1)} %reshape.388), calls=%async_computation.4 | async-start | bytes 65536 | tf_op jit(solution)/shard_map/all_to_all | solution.py:180
  102.0 0.7 copy-start.8
  103.7 4.5 %copy-start.4 = (bf16[16,1024]{1,0:T(8,128)(2,1)S(1)}, bf16[16,1024]{1,0:T(8,128)(2,1)}, u32[]{:S(2)}) copy-start(bf16[16,1024]{1,0:T(8,128)(2,1)} %param.29) | copy-start | bytes 98308
  103.7 13.6 %all-to-all-start.5 = ((bf16[4,2,2048]{2,1,0:T(2,128)(2,1)}), bf16[4,2,2048]{2,1,0:T(2,128)(2,1)S(1)}, u32[]{:S(2)}, u32[]{:S(2)}) async-start(bf16[4,2,2048]{2,1,0:T(2,128)(2,1)} %reshape.390), calls=%async_computation.5 | async-start | bytes 65536 | tf_op jit(solution)/shard_map/all_to_all | solution.py:193
